TPU v7x, 32 devices: a whole 2x2x4 slice. The times are simulated.
32 devices in a mesh: sp: 8 (over z, x), tp: 4 (over y, core).
Axes of the slice: x: 2, y: 2, z: 4, core: 2. Of those that a mesh axis runs over, the one named last changes fastest.
Arguments:
- tokens: bfloat16 [1024, 1024], P('sp', 'tp'), may hold values from -6 to 6
- norm_gain: float32 [3, 1024], replicated, may hold values from 0.1 to 1.9
- w_query: bfloat16 [3, 1024, 1024], P(None, 'sp', 'tp'), may hold values from -0.1875 to 0.1875
- w_key: bfloat16 [3, 1024, 1024], P(None, 'sp', 'tp'), may hold values from -0.1875 to 0.1875
- w_value: bfloat16 [3, 1024, 1024], P(None, 'sp', 'tp'), may hold values from -0.1875 to 0.1875
- w_out: bfloat16 [3, 1024, 1024], P(None, 'tp', 'sp'), may hold values from -0.5625 to 0.5625
- offset_bias: float32 [3, 16, 8, 16], P(None, 'tp'), may hold values from -3 to 3
- documents: int32 [1024], P('sp'), may hold values from 0 to 7, never falling along the last dimension, each value on 1 to 256 neighbouring positions
Outputs:
- mixed: bfloat16 [1024, 1024], P('sp', 'tp')
Inputs may be any that keep to these rules, and one draw needn't show every extreme that they name: `documents`: document numbers never fall along the token order, start at 0, and each document has 1 to 256 tokens.
All inputs are finite; a program needn't handle non-finite values.
Results may differ from a plain program's by a relative error of at most 0.02.
Values may be sent and summed in bfloat16 or wider, within the bound.
A program may use at most 64 MiB of HBM per device.

v0:
```python
import jax
import jax.numpy as jnp
from jax import lax
from jax.sharding import PartitionSpec as P

HEAD_DIM = 64
WIN_ROWS = 8
WIN_COLS = 16
LAYERS = 3
GRID_W = 32
EPS = 1e-06


def with_halo(shard, sides, width, wrap):
    for axis, dim in sides:
        count, length = (lax.axis_size(axis), shard.shape[dim])
        up = [(i, (i + 1) % count) for i in range(count if wrap else count - 1)]
        down = [(j, i) for i, j in up]
        last = lax.slice_in_dim(shard, length - width, length, axis=dim)
        leading = lax.slice_in_dim(shard, 0, width, axis=dim)
        before = lax.ppermute(last, axis, up)
        after = lax.ppermute(leading, axis, down)
        shard = jnp.concatenate([before, shard, after], axis=dim)
    return shard


def rms_rows(stream, gain_row):
    values = stream.astype(jnp.float32)
    mean_sq = jnp.mean(values * values, axis=-1, keepdims=True)
    return (values * lax.rsqrt(mean_sq + EPS) * gain_row).astype(jnp.bfloat16)


def head_norm(heads_raw):
    values = heads_raw.astype(jnp.float32)
    mean_sq = jnp.mean(values * values, axis=-1, keepdims=True)
    return (values * lax.rsqrt(mean_sq + EPS)).astype(jnp.bfloat16)


def attend(queries, fringe, seg_own, seg_fringe, bias_layer):
    row_count, grid_width, head_count, head_width = queries.shape
    key_rows = jnp.stack(
        [fringe[row_lag : row_lag + row_count] for row_lag in range(WIN_ROWS)], axis=1
    )
    seg_rows = jnp.stack(
        [seg_fringe[row_lag : row_lag + row_count] for row_lag in range(WIN_ROWS)], axis=1
    )
    key_part = key_rows[..., :head_width]
    value_part = key_rows[..., head_width:]
    scores = jnp.einsum(
        "rchd,rjkhd->rhcjk", queries, key_part, preferred_element_type=jnp.float32
    ) * head_width ** (-0.5)
    column = jnp.arange(grid_width)
    col_offset = column[None, :] - column[:, None] + WIN_COLS // 2
    inside = (col_offset >= 0) & (col_offset < WIN_COLS)
    bias_table = bias_layer[:, :, jnp.clip(col_offset, 0, WIN_COLS - 1)]
    scores = scores + jnp.transpose(bias_table, (0, 2, 1, 3))[None]
    same_doc = seg_rows[:, None, None, :, :] == seg_own[:, None, :, None, None]
    allowed = same_doc & inside[None, None, :, None, :]
    scores = jnp.where(allowed, scores, -1e30)
    flat = scores.reshape(row_count, head_count, grid_width, WIN_ROWS * grid_width)
    attn_probs = jax.nn.softmax(flat, axis=-1).astype(jnp.bfloat16)
    attn_probs = attn_probs.reshape(row_count, head_count, grid_width, WIN_ROWS, grid_width)
    mixed_heads = jnp.einsum(
        "rhcjk,rjkhd->rchd", attn_probs, value_part, preferred_element_type=jnp.float32
    )
    return mixed_heads.astype(jnp.bfloat16)


def body(tokens, norm_gain, w_query, w_key, w_value, w_out, offset_bias, documents):
    token_count = tokens.shape[0]
    row_count = token_count // GRID_W
    reach_rows = WIN_ROWS // 2
    head_count = offset_bias.shape[1]
    seg_own = (documents + 1).reshape(row_count, GRID_W)
    seg_fringe = with_halo(seg_own, (("sp", 0),), reach_rows, False)
    collected = (
        lax.all_gather(w_query, "sp", axis=1, tiled=True),
        lax.all_gather(w_key, "sp", axis=1, tiled=True),
        lax.all_gather(w_value, "sp", axis=1, tiled=True),
        lax.all_gather(w_out, "sp", axis=2, tiled=True),
    )
    stream = tokens
    for layer_index in range(LAYERS):
        gathered = lax.all_gather(stream, "tp", axis=1, tiled=True)
        normed = rms_rows(gathered, norm_gain[layer_index])
        query_raw = jnp.dot(normed, collected[0][layer_index], preferred_element_type=jnp.float32)
        key_raw = jnp.dot(normed, collected[1][layer_index], preferred_element_type=jnp.float32)
        value_raw = jnp.dot(normed, collected[2][layer_index], preferred_element_type=jnp.float32)
        query_heads = head_norm(
            query_raw.astype(jnp.bfloat16).reshape(row_count, GRID_W, head_count, HEAD_DIM)
        )
        key_heads = head_norm(
            key_raw.astype(jnp.bfloat16).reshape(row_count, GRID_W, head_count, HEAD_DIM)
        )
        value_heads = value_raw.astype(jnp.bfloat16).reshape(
            row_count, GRID_W, head_count, HEAD_DIM
        )
        key_value = jnp.concatenate([key_heads, value_heads], axis=-1)
        fringe = with_halo(key_value, (("sp", 0),), reach_rows, False)
        attended = attend(query_heads, fringe, seg_own, seg_fringe, offset_bias[layer_index])
        attended = attended.reshape(token_count, head_count * HEAD_DIM)
        partial_sums = jnp.dot(
            attended, collected[3][layer_index], preferred_element_type=jnp.float32
        )
        stream = (
            lax.psum_scatter(
                partial_sums.astype(jnp.bfloat16), "tp", scatter_dimension=1, tiled=True
            )
            .astype(jnp.float32)
            .astype(jnp.bfloat16)
        )
    return stream


def solution(mesh):
    return jax.shard_map(
        body,
        mesh=mesh,
        in_specs=(
            P("sp", "tp"),
            P(),
            P(None, "sp", "tp"),
            P(None, "sp", "tp"),
            P(None, "sp", "tp"),
            P(None, "tp", "sp"),
            P(None, "tp", None, None),
            P("sp"),
        ),
        out_specs=P("sp", "tp"),
        check_vma=False,
    )
```

profile of v0, /device:TPU:0, one launch (start us, length us, event | category | flops | bytes accessed | tf_op | source)
XLA Modules:
  0.0 309.1 jit_solution(167499018848324964)
XLA Ops:
  9.5 4.9 %collective-permute-start.2 = (s32[4,32]{1,0:T(4,128)S(1)}, s32[4,32]{1,0:T(4,128)S(1)}, u32[]{:S(2)}, u32[]{:S(2)}) collective-permute-start(s32[4,32]{1,0:T(4,128)S(1)} %reshape.186), channel_id=1, source_target_pairs={{0,4},{4,8},{8,12},{12,16},{16,20},{20,24},{24,28},{1,5},{5,9},{9,... | collective-permute-start | bytes 1544 | tf_op jit(solution)/shard_map/ppermute | solution.py:21
  15.8 6.0 %all_gather.21 = bf16[128,1024]{1,0:T(8,128)(2,1)S(1)} all-gather(bf16[128,256]{1,0:T(8,128)(2,1)} %param.8), channel_id=1, replica_groups=mesh['sp'=8,'tp'=4] {'tp'}, dimensions={1}, use_global_device_ids=true | all-gather | bytes 327680 | tf_op jit(solution)/shard_map/all_gather | solution.py:84
  23.8 3.5 %gather_fusion = f32[1024,4,8]{2,1,0:T(4,128)S(1)} fusion(f32[4,8,16]{1,0,2:T(4,128)S(1)} %bitcast.251, s32[1024]{0:T(1024)S(1)} %broadcast_clamp_fusion), kind=kCustom, calls=%fused_computation | custom fusion | bytes 266240 | tf_op jit(solution)/shard_map/gather | solution.py:55
  29.0 27.4 %all-gather.5.cloned.1.call-done = bf16[3,1024,256]{2,1,0:T(8,128)(2,1)} async-done(((bf16[3,128,256]{2,1,0:T(8,128)(2,1)}), bf16[3,1024,256]{2,1,0:T(8,128)(2,1)}) %all-gather.5.cloned.1.call-update) | async-done | bytes 1572880 | tf_op jit(solution)/shard_map/all_gather | solution.py:78
  56.4 1.3 fusion.17
  58.4 42.8 %all-gather.7.cloned.1.call-done = bf16[3,1024,256]{2,1,0:T(8,128)(2,1)} async-done(((bf16[3,128,256]{2,1,0:T(8,128)(2,1)}), bf16[3,1024,256]{2,1,0:T(8,128)(2,1)}) %all-gather.7.cloned.1.call-update) | async-done | bytes 1572880 | tf_op jit(solution)/shard_map/all_gather | solution.py:79
  101.2 1.3 convolution_convert_fusion.10
  102.8 2.5 collective-permute-start
  106.5 39.4 %all-gather.9.cloned.1.call-done = bf16[3,1024,256]{2,1,0:T(8,128)(2,1)} async-done(((bf16[3,128,256]{2,1,0:T(8,128)(2,1)}), bf16[3,1024,256]{2,1,0:T(8,128)(2,1)}) %all-gather.9.cloned.1.call-update) | async-done | bytes 1572880 | tf_op jit(solution)/shard_map/all_gather | solution.py:77
  146.0 1.3 fusion.16
  150.8 39.8 %all-gather.11.cloned.1.call-done = bf16[3,256,1024]{2,1,0:T(8,128)(2,1)} async-done(((bf16[3,256,128]{2,1,0:T(8,128)(2,1)}), bf16[3,256,1024]{2,1,0:T(8,128)(2,1)}) %all-gather.11.cloned.1.call-update) | async-done | bytes 1572880 | tf_op jit(solution)/shard_map/all_gather | solution.py:80
  190.7 2.0 convolution_convert_fusion.2
  192.8 3.6 %gather_fusion.1 = f32[1024,4,8]{2,1,0:T(4,128)S(1)} fusion(f32[4,8,16]{1,0,2:T(4,128)S(1)} %bitcast.252, s32[1024]{0:T(1024)S(1)} %broadcast_clamp_fusion), kind=kCustom, calls=%fused_computation.1 | custom fusion | bytes 266240 | tf_op jit(solution)/shard_map/gather | solution.py:55
  197.6 13.6 %reduce-scatter.4.cloned.1.call-done = bf16[128,256]{1,0:T(8,128)(2,1)} async-done(((bf16[128,1024]{1,0:T(8,128)(2,1)}), bf16[128,256]{1,0:T(8,128)(2,1)}) %reduce-scatter.4.cloned.1.call-update) | async-done | bytes 65552 | tf_op jit(solution)/shard_map/reduce_scatter | solution.py:106
  211.2 6.0 %all_gather.26 = bf16[128,1024]{1,0:T(8,128)(2,1)S(1)} all-gather(bf16[128,256]{1,0:T(8,128)(2,1)} %reduce-scatter.4.cloned.1.call-done), channel_id=1, replica_groups=mesh['sp'=8,'tp'=4] {'tp'}, dimensions={1}, use_global_device_ids=true | all-gather | bytes 327680 | tf_op jit(solution)/shard_map/all_gather | solution.py:84
  217.4 1.3 fusion.15
  219.3 1.3 convolution_convert_fusion.7
  220.9 3.4 %collective-permute-start.4 = (bf16[4,32,4,128]{3,1,2,0:T(8,128)(2,1)S(1)}, bf16[4,32,4,128]{3,1,2,0:T(8,128)(2,1)S(1)}, u32[]{:S(2)}, u32[]{:S(2)}) collective-permute-start(bf16[4,32,4,128]{3,1,2,0:T(8,128)(2,1)S(1)} %pad_maximum_fusion.4), channel_id=1, source_target_pairs={{0,4},{4,8},{8,12},{12,16},{16,20},{20,24},{24,28},{1,5},{5,9},{9,... | collective-permute-start | bytes 393224 | tf_op jit(solution)/shard_map/ppermute | solution.py:21
  224.3 1.5 collective-permute-start.5
  225.8 1.3 fusion.14
  227.7 3.9 %collective-permute-done.5 = bf16[4,32,4,128]{3,1,2,0:T(8,128)(2,1)S(1)} collective-permute-done((bf16[4,32,4,128]{3,1,2,0:T(8,128)(2,1)S(1)}, bf16[4,32,4,128]{3,1,2,0:T(8,128)(2,1)S(1)}, u32[]{:S(2)}, u32[]{:S(2)}) %collective-permute-start.5) | collective-permute-done | bytes 131104 | tf_op jit(solution)/shard_map/ppermute | solution.py:22
  234.6 2.0 convolution_convert_fusion.1
  236.7 3.5 %gather_fusion.2 = f32[1024,4,8]{2,1,0:T(4,128)S(1)} fusion(f32[4,8,16]{1,0,2:T(4,128)S(1)} %bitcast.250, s32[1024]{0:T(1024)S(1)} %broadcast_clamp_fusion), kind=kCustom, calls=%fused_computation.2 | custom fusion | bytes 266240 | tf_op jit(solution)/shard_map/gather | solution.py:55
  241.5 15.2 %reduce-scatter.6.cloned.1.call-done = bf16[128,256]{1,0:T(8,128)(2,1)} async-done(((bf16[128,1024]{1,0:T(8,128)(2,1)}), bf16[128,256]{1,0:T(8,128)(2,1)}) %reduce-scatter.6.cloned.1.call-update) | async-done | bytes 65552 | tf_op jit(solution)/shard_map/reduce_scatter | solution.py:106
  256.7 6.0 %all_gather.27 = bf16[128,1024]{1,0:T(8,128)(2,1)S(1)} all-gather(bf16[128,256]{1,0:T(8,128)(2,1)} %reduce-scatter.6.cloned.1.call-done), channel_id=1, replica_groups=mesh['sp'=8,'tp'=4] {'tp'}, dimensions={1}, use_global_device_ids=true | all-gather | bytes 327680 | tf_op jit(solution)/shard_map/all_gather | solution.py:84
  262.9 1.3 fusion.13
  264.8 1.3 convolution_convert_fusion.4
  266.4 3.4 %collective-permute-start.6 = (bf16[4,32,4,128]{3,1,2,0:T(8,128)(2,1)S(1)}, bf16[4,32,4,128]{3,1,2,0:T(8,128)(2,1)S(1)}, u32[]{:S(2)}, u32[]{:S(2)}) collective-permute-start(bf16[4,32,4,128]{3,1,2,0:T(8,128)(2,1)S(1)} %pad_maximum_fusion.5), channel_id=1, source_target_pairs={{0,4},{4,8},{8,12},{12,16},{16,20},{20,24},{24,28},{1,5},{5,9},{9,... | collective-permute-start | bytes 393224 | tf_op jit(solution)/shard_map/ppermute | solution.py:21
  271.1 1.3 fusion.12
  273.1 4.1 %collective-permute-done.7 = bf16[4,32,4,128]{3,1,2,0:T(8,128)(2,1)S(1)} collective-permute-done((bf16[4,32,4,128]{3,1,2,0:T(8,128)(2,1)S(1)}, bf16[4,32,4,128]{3,1,2,0:T(8,128)(2,1)S(1)}, u32[]{:S(2)}, u32[]{:S(2)}) %collective-permute-start.7) | collective-permute-done | bytes 131104 | tf_op jit(solution)/shard_map/ppermute | solution.py:22
  280.1 2.0 convolution_convert_fusion
  282.1 20.2 %reduce-scatter.8.cloned.1.call-done = bf16[128,256]{1,0:T(8,128)(2,1)} async-done(((bf16[128,1024]{1,0:T(8,128)(2,1)}), bf16[128,256]{1,0:T(8,128)(2,1)}) %reduce-scatter.8.cloned.1.call-update) | async-done | bytes 65552 | tf_op jit(solution)/shard_map/reduce_scatter | solution.py:106
  (133 shorter events, 26.4 us)
Async XLA Ops:
  6.5 49.9 %all-gather.5.cloned.1.call-start = ((), (), s32[]{:S(2)}) async-start(), calls=%async_computation.3 | async-start | bytes 1769472 | tf_op jit(solution)/shard_map/all_gather | solution.py:78
  7.3 93.9 %all-gather.7.cloned.1.call-start = ((), (), s32[]{:S(2)}) async-start(), calls=%async_computation.4 | async-start | bytes 1769472 | tf_op jit(solution)/shard_map/all_gather | solution.py:79
  8.0 137.9 %all-gather.9.cloned.1.call-start = ((), (), s32[]{:S(2)}) async-start(), calls=%async_computation.5 | async-start | bytes 1769472 | tf_op jit(solution)/shard_map/all_gather | solution.py:77
  8.7 181.9 %all-gather.11.cloned.1.call-start = ((), (), s32[]{:S(2)}) async-start(), calls=%async_computation.6 | async-start | bytes 1769472 | tf_op jit(solution)/shard_map/all_gather | solution.py:80
  9.5 19.1 %collective-permute-start.2 = (s32[4,32]{1,0:T(4,128)S(1)}, s32[4,32]{1,0:T(4,128)S(1)}, u32[]{:S(2)}, u32[]{:S(2)}) collective-permute-start(s32[4,32]{1,0:T(4,128)S(1)} %reshape.186), channel_id=1, source_target_pairs={{0,4},{4,8},{8,12},{12,16},{16,20},{20,24},{24,28},{1,5},{5,9},{9,... | collective-permute-start | bytes 1544 | tf_op jit(solution)/shard_map/ppermute | solution.py:21
  14.4 14.2 %collective-permute-start.3 = (s32[4,32]{1,0:T(4,128)S(1)}, s32[4,32]{1,0:T(4,128)S(1)}, u32[]{:S(2)}, u32[]{:S(2)}) collective-permute-start(s32[4,32]{1,0:T(4,128)S(1)} %reshape.186), channel_id=1, source_target_pairs={{4,0},{8,4},{12,8},{16,12},{20,16},{24,20},{28,24},{5,1},{9,5},{13... | collective-permute-start | bytes 1544 | tf_op jit(solution)/shard_map/ppermute | solution.py:22
  15.7 195.5 %reduce-scatter.4.cloned.1.call-start = ((), (), s32[]{:S(2)}) async-start(), calls=%async_computation.7 | async-start | bytes 327680 | tf_op jit(solution)/shard_map/reduce_scatter | solution.py:106
  102.8 45.1 %collective-permute-start = (bf16[4,32,4,128]{3,1,2,0:T(8,128)(2,1)S(1)}, bf16[4,32,4,128]{3,1,2,0:T(8,128)(2,1)S(1)}, u32[]{:S(2)}, u32[]{:S(2)}) collective-permute-start(bf16[4,32,4,128]{3,1,2,0:T(8,128)(2,1)S(1)} %pad_maximum_fusion.3), channel_id=1, source_target_pairs={{0,4},{4,8},{8,12},{12,16},{16,20},{20,24},{24,28},{1,5},{5,9},{9,... | collective-permute-start | bytes 393224 | tf_op jit(solution)/shard_map/ppermute | solution.py:21
  105.2 42.7 %collective-permute-start.1 = (bf16[4,32,4,128]{3,1,2,0:T(8,128)(2,1)S(1)}, bf16[4,32,4,128]{3,1,2,0:T(8,128)(2,1)S(1)}, u32[]{:S(2)}, u32[]{:S(2)}) collective-permute-start(bf16[4,32,4,128]{3,1,2,0:T(8,128)(2,1)S(1)} %pad_maximum_fusion.3), channel_id=1, source_target_pairs={{4,0},{8,4},{12,8},{16,12},{20,16},{24,20},{28,24},{5,1},{9,5},{13... | collective-permute-start | bytes 393224 | tf_op jit(solution)/shard_map/ppermute | solution.py:22
  192.7 64.1 %reduce-scatter.6.cloned.1.call-start = ((), (), s32[]{:S(2)}) async-start(), calls=%async_computation.8 | async-start | bytes 327680 | tf_op jit(solution)/shard_map/reduce_scatter | solution.py:106
  220.9 6.8 %collective-permute-start.4 = (bf16[4,32,4,128]{3,1,2,0:T(8,128)(2,1)S(1)}, bf16[4,32,4,128]{3,1,2,0:T(8,128)(2,1)S(1)}, u32[]{:S(2)}, u32[]{:S(2)}) collective-permute-start(bf16[4,32,4,128]{3,1,2,0:T(8,128)(2,1)S(1)} %pad_maximum_fusion.4), channel_id=1, source_target_pairs={{0,4},{4,8},{8,12},{12,16},{16,20},{20,24},{24,28},{1,5},{5,9},{9,... | collective-permute-start | bytes 393224 | tf_op jit(solution)/shard_map/ppermute | solution.py:21
  224.3 7.4 %collective-permute-start.5 = (bf16[4,32,4,128]{3,1,2,0:T(8,128)(2,1)S(1)}, bf16[4,32,4,128]{3,1,2,0:T(8,128)(2,1)S(1)}, u32[]{:S(2)}, u32[]{:S(2)}) collective-permute-start(bf16[4,32,4,128]{3,1,2,0:T(8,128)(2,1)S(1)} %pad_maximum_fusion.4), channel_id=1, source_target_pairs={{4,0},{8,4},{12,8},{16,12},{20,16},{24,20},{28,24},{5,1},{9,5},{13... | collective-permute-start | bytes 393224 | tf_op jit(solution)/shard_map/ppermute | solution.py:22
  236.6 65.7 %reduce-scatter.8.cloned.1.call-start = ((), (), s32[]{:S(2)}) async-start(), calls=%async_computation.9 | async-start | bytes 327680 | tf_op jit(solution)/shard_map/reduce_scatter | solution.py:106
  266.4 6.6 %collective-permute-start.6 = (bf16[4,32,4,128]{3,1,2,0:T(8,128)(2,1)S(1)}, bf16[4,32,4,128]{3,1,2,0:T(8,128)(2,1)S(1)}, u32[]{:S(2)}, u32[]{:S(2)}) collective-permute-start(bf16[4,32,4,128]{3,1,2,0:T(8,128)(2,1)S(1)} %pad_maximum_fusion.5), channel_id=1, source_target_pairs={{0,4},{4,8},{8,12},{12,16},{16,20},{20,24},{24,28},{1,5},{5,9},{9,... | collective-permute-start | bytes 393224 | tf_op jit(solution)/shard_map/ppermute | solution.py:21
  269.8 7.4 %collective-permute-start.7 = (bf16[4,32,4,128]{3,1,2,0:T(8,128)(2,1)S(1)}, bf16[4,32,4,128]{3,1,2,0:T(8,128)(2,1)S(1)}, u32[]{:S(2)}, u32[]{:S(2)}) collective-permute-start(bf16[4,32,4,128]{3,1,2,0:T(8,128)(2,1)S(1)} %pad_maximum_fusion.5), channel_id=1, source_target_pairs={{4,0},{8,4},{12,8},{16,12},{20,16},{24,20},{28,24},{5,1},{9,5},{13... | collective-permute-start | bytes 393224 | tf_op jit(solution)/shard_map/ppermute | solution.py:22
Sparse Core Ops, SparseCore 0:
  9.5 46.8 all-gather.4
  58.6 42.5 all-gather.6
  103.4 42.5 all-gather.8
  147.8 42.7 all-gather.10
  193.0 18.2 reduce-scatter.3
  236.7 19.9 reduce-scatter.5
  282.2 20.0 reduce-scatter.7
where the time goes:
time: 310 us; the launch traced here: 309 us
  waiting for transfers between devices  209 us (67%)
  matrix products  23 us (7%)
  starting transfers between devices  19.7 us (6%)
  local copies, waits for them, and re-layouts  19.3 us (6%)
  blocking collectives  17.9 us (6%)
  between operations  14.2 us (5%)
  other arithmetic  6.3 us (2%)
    reduce_scatter x3, waiting for transfers between devices, body(): lax.psum_scatter(partial_sums.astype(jnp.bfloat16), 'tp', scatter_dimensi...  49 us
    all_gather x1, waiting for transfers between devices, body(): lax.all_gather(w_value, 'sp', axis=1, tiled=True)  42.8 us
    all_gather x1, waiting for transfers between devices, body(): lax.all_gather(w_out, 'sp', axis=2, tiled=True)  39.8 us
    all_gather x1, waiting for transfers between devices, body(): lax.all_gather(w_query, 'sp', axis=1, tiled=True)  39.4 us
    all_gather x1, waiting for transfers between devices, body(): lax.all_gather(w_key, 'sp', axis=1, tiled=True)  27.4 us
    all_gather x3, blocking collectives, body(): gathered = lax.all_gather(stream, 'tp', axis=1, tiled=True)  17.9 us
    gather x6, local copies, waits for them, and re-layouts, attend(): bias_table = bias_layer[:, :, jnp.clip(col_offset, 0, WIN_COLS - 1)]  14.4 us
    ppermute x4, starting transfers between devices, with_halo(): before = lax.ppermute(last, axis, up)  14.1 us
  transfers between devices with their start and end apart: 15, of which 9 were waited for; matrix products, arithmetic and copies ran while one was open for 10% of the time, Pallas kernels for 0%

commit v1 on v0

--- a/solution.py
+++ b/solution.py
@@ -9,6 +9,22 @@
 LAYERS = 3
 GRID_W = 32
 EPS = 1e-06
+
+
+def collect(x, axis, dim):
+    ways, here, hop = (lax.axis_size(axis), lax.axis_index(axis), x.shape[dim])
+    shape = [n * ways if d == dim else n for d, n in enumerate(x.shape)]
+    full = lax.dynamic_update_slice_in_dim(jnp.zeros(shape, x.dtype), x, here * hop, axis=dim)
+    going_up = going_down = x
+    for far in range(1, ways // 2 + 1):
+        going_up = lax.ppermute(going_up, axis, [(d, (d + 1) % ways) for d in range(ways)])
+        full = lax.dynamic_update_slice_in_dim(full, going_up, (here - far) % ways * hop, axis=dim)
+        if 2 * far < ways:
+            going_down = lax.ppermute(going_down, axis, [(d, (d - 1) % ways) for d in range(ways)])
+            full = lax.dynamic_update_slice_in_dim(
+                full, going_down, (here + far) % ways * hop, axis=dim
+            )
+    return full
 
 
 def with_halo(shard, sides, width, wrap):
@@ -77,7 +93,7 @@
         lax.all_gather(w_query, "sp", axis=1, tiled=True),
         lax.all_gather(w_key, "sp", axis=1, tiled=True),
         lax.all_gather(w_value, "sp", axis=1, tiled=True),
-        lax.all_gather(w_out, "sp", axis=2, tiled=True),
+        collect(w_out, "sp", 2),
     )
     stream = tokens
     for layer_index in range(LAYERS):

time: 310 us -> 279 us (0.900)
  waiting for transfers between devices: 209 us -> 150 us
  local copies, waits for them, and re-layouts: 19.3 us -> 37.1 us
  starting transfers between devices: 19.7 us -> 32.2 us
  matrix products: 23 us -> 19.9 us
    all_gather x1 -> x0, waiting for transfers between devices: 39.8 us -> none  [body(): lax.all_gather(w_out, 'sp', axis=2, tiled=True)]
    ppermute x0 -> x7, waiting for transfers between devices: none -> 28.7 us  [the longest x4 28.2 us: collect(): lax.ppermute(going_up, axis, [(d, (d + 1) % ways) for d in range(ways)])]
    all_gather x1, waiting for transfers between devices: 27.4 us -> 0.02 us  [body(): lax.all_gather(w_key, 'sp', axis=1, tiled=True)]
    gather x6, local copies, waits for them, and re-layouts: 14.4 us -> 30.9 us  [attend(): bias_table = bias_layer[:, :, jnp.clip(col_offset, 0, WIN_COLS - 1)]]
    ppermute x0 -> x7, starting transfers between devices: none -> 16.2 us  [the longest x4 8.2 us: collect(): lax.ppermute(going_up, axis, [(d, (d + 1) % ways) for d in range(ways)])]
    reduce_scatter x3, waiting for transfers between devices: 49 us -> 38.1 us  [body(): lax.psum_scatter(partial_sums.astype(jnp.bfloat16), 'tp', scatter_dimensi...]
    all_gather x1, waiting for transfers between devices: 42.8 us -> 34.5 us  [body(): lax.all_gather(w_value, 'sp', axis=1, tiled=True)]
    ppermute x4, starting transfers between devices: 14.1 us -> 10.5 us  [with_halo(): before = lax.ppermute(last, axis, up)]
  transfers between devices with their start and end apart: 15 -> 21, of which waited for: 9 -> 11; matrix products, arithmetic and copies ran while one was open for 10% -> 16% of each run, Pallas kernels for 0% -> 0%
where the time goes in v1:
time: 279 us; the launch traced here: 278 us
  waiting for transfers between devices  150 us (54%)
  local copies, waits for them, and re-layouts  37.1 us (13%)
  starting transfers between devices  32.2 us (12%)
  matrix products  19.9 us (7%)
  blocking collectives  18.1 us (6%)
  between operations  14.5 us (5%)
  other arithmetic  6.3 us (2%)
    all_gather x1, waiting for transfers between devices, body(): lax.all_gather(w_query, 'sp', axis=1, tiled=True)  39.1 us
    reduce_scatter x3, waiting for transfers between devices, body(): lax.psum_scatter(partial_sums.astype(jnp.bfloat16), 'tp', scatter_dimensi...  38.1 us
    all_gather x1, waiting for transfers between devices, body(): lax.all_gather(w_value, 'sp', axis=1, tiled=True)  34.5 us
    gather x6, local copies, waits for them, and re-layouts, attend(): bias_table = bias_layer[:, :, jnp.clip(col_offset, 0, WIN_COLS - 1)]  30.9 us
    ppermute x4, waiting for transfers between devices, collect(): lax.ppermute(going_up, axis, [(d, (d + 1) % ways) for d in range(ways)])  28.2 us
    all_gather x3, blocking collectives, body(): gathered = lax.all_gather(stream, 'tp', axis=1, tiled=True)  18.1 us
    ppermute x4, starting transfers between devices, with_halo(): before = lax.ppermute(last, axis, up)  10.5 us
    ppermute x4, starting transfers between devices, collect(): lax.ppermute(going_up, axis, [(d, (d + 1) % ways) for d in range(ways)])  8.2 us
  transfers between devices with their start and end apart: 21, of which 11 were waited for; matrix products, arithmetic and copies ran while one was open for 16% of the time, Pallas kernels for 0%

profile of v1, /device:TPU:0, one launch (start us, length us, event | category | flops | bytes accessed | tf_op | source)
XLA Modules:
  0.0 278.0 jit_solution(7077425457252639507)
XLA Ops:
  8.1 3.0 %collective-permute-start.4 = (bf16[3,256,128]{2,1,0:T(8,128)(2,1)}, bf16[3,256,128]{2,1,0:T(8,128)(2,1)S(1)}, u32[]{:S(2)}, u32[]{:S(2)}) collective-permute-start(bf16[3,256,128]{2,1,0:T(8,128)(2,1)} %param.13), channel_id=1, source_target_pairs={{0,4},{4,8},{8,12},{12,16},{16,20},{20,24},{24,28},{28,0},{1,5},{5... | collective-permute-start | bytes 589832 | tf_op jit(solution)/shard_map/ppermute | solution.py:20
  11.1 3.1 %collective-permute-start.5 = (bf16[3,256,128]{2,1,0:T(8,128)(2,1)}, bf16[3,256,128]{2,1,0:T(8,128)(2,1)S(1)}, u32[]{:S(2)}, u32[]{:S(2)}) collective-permute-start(bf16[3,256,128]{2,1,0:T(8,128)(2,1)} %param.13), channel_id=1, source_target_pairs={{0,28},{4,0},{8,4},{12,8},{16,12},{20,16},{24,20},{28,24},{1,29},{... | collective-permute-start | bytes 589832 | tf_op jit(solution)/shard_map/ppermute | solution.py:23
  17.8 6.1 %all_gather.18 = bf16[128,1024]{1,0:T(8,128)(2,1)S(1)} all-gather(bf16[128,256]{1,0:T(8,128)(2,1)} %param.8), channel_id=1, replica_groups=mesh['sp'=8,'tp'=4] {'tp'}, dimensions={1}, use_global_device_ids=true | all-gather | bytes 327680 | tf_op jit(solution)/shard_map/all_gather | solution.py:100
  24.9 1.4 fusion.78
  26.7 7.9 %gather_fusion = f32[1024,4,8]{2,1,0:T(4,128)} fusion(f32[4,8,16]{1,0,2:T(4,128)S(1)} %bitcast.250, s32[1024]{0:T(1024)S(1)} %broadcast_clamp_fusion), kind=kCustom, calls=%fused_computation | custom fusion | bytes 266240 | tf_op jit(solution)/shard_map/gather | solution.py:71
  34.7 2.4 copy.150
  37.5 2.7 collective-permute-start.6
  40.2 2.5 collective-permute-start.7
  42.8 10.9 %collective-permute-done.6 = bf16[3,256,128]{2,1,0:T(8,128)(2,1)S(1)} collective-permute-done((bf16[3,256,128]{2,1,0:T(8,128)(2,1)S(1)}, bf16[3,256,128]{2,1,0:T(8,128)(2,1)S(1)}, u32[]{:S(2)}, u32[]{:S(2)}) %collective-permute-start.6) | collective-permute-done | bytes 196640 | tf_op jit(solution)/shard_map/ppermute | solution.py:20
  53.7 2.5 collective-permute-start.8
  56.7 2.4 collective-permute-start.9
  59.2 8.8 %collective-permute-done.8 = bf16[3,256,128]{2,1,0:T(8,128)(2,1)S(1)} collective-permute-done((bf16[3,256,128]{2,1,0:T(8,128)(2,1)S(1)}, bf16[3,256,128]{2,1,0:T(8,128)(2,1)S(1)}, u32[]{:S(2)}, u32[]{:S(2)}) %collective-permute-start.8) | collective-permute-done | bytes 196640 | tf_op jit(solution)/shard_map/ppermute | solution.py:20
  68.2 8.5 %collective-permute-done.10 = bf16[3,256,128]{2,1,0:T(8,128)(2,1)S(1)} collective-permute-done((bf16[3,256,128]{2,1,0:T(8,128)(2,1)S(1)}, bf16[3,256,128]{2,1,0:T(8,128)(2,1)S(1)}, u32[]{:S(2)}, u32[]{:S(2)}) %collective-permute-start.10) | collective-permute-done | bytes 196640 | tf_op jit(solution)/shard_map/ppermute | solution.py:20
  76.8 1.3 fusion.17
  78.6 34.5 %all-gather.6.cloned.1.call-done = bf16[3,1024,256]{2,1,0:T(8,128)(2,1)} async-done(((bf16[3,128,256]{2,1,0:T(8,128)(2,1)}), bf16[3,1024,256]{2,1,0:T(8,128)(2,1)}) %all-gather.6.cloned.1.call-update) | async-done | bytes 1572880 | tf_op jit(solution)/shard_map/all_gather | solution.py:95
  114.8 2.5 collective-permute-start
  118.6 39.1 %all-gather.8.cloned.1.call-done = bf16[3,1024,256]{2,1,0:T(8,128)(2,1)} async-done(((bf16[3,128,256]{2,1,0:T(8,128)(2,1)}), bf16[3,1024,256]{2,1,0:T(8,128)(2,1)}) %all-gather.8.cloned.1.call-update) | async-done | bytes 1572880 | tf_op jit(solution)/shard_map/all_gather | solution.py:93
  157.7 1.3 fusion.16
  163.7 7.9 %gather_fusion.1 = f32[1024,4,8]{2,1,0:T(4,128)} fusion(f32[4,8,16]{1,0,2:T(4,128)S(1)} %bitcast.252, s32[1024]{0:T(1024)S(1)} %broadcast_clamp_fusion), kind=kCustom, calls=%fused_computation.1 | custom fusion | bytes 266240 | tf_op jit(solution)/shard_map/gather | solution.py:71
  171.7 2.4 copy.167
  174.0 8.1 %reduce-scatter.4.cloned.1.call-done = bf16[128,256]{1,0:T(8,128)(2,1)} async-done(((bf16[128,1024]{1,0:T(8,128)(2,1)}), bf16[128,256]{1,0:T(8,128)(2,1)}) %reduce-scatter.4.cloned.1.call-update) | async-done | bytes 65552 | tf_op jit(solution)/shard_map/reduce_scatter | solution.py:122
  182.1 6.0 %all_gather.22 = bf16[128,1024]{1,0:T(8,128)(2,1)S(1)} all-gather(bf16[128,256]{1,0:T(8,128)(2,1)} %reduce-scatter.4.cloned.1.call-done), channel_id=1, replica_groups=mesh['sp'=8,'tp'=4] {'tp'}, dimensions={1}, use_global_device_ids=true | all-gather | bytes 327680 | tf_op jit(solution)/shard_map/all_gather | solution.py:100
  191.8 3.4 %collective-permute-start.11 = (bf16[4,32,4,128]{3,1,2,0:T(8,128)(2,1)S(1)}, bf16[4,32,4,128]{3,1,2,0:T(8,128)(2,1)S(1)}, u32[]{:S(2)}, u32[]{:S(2)}) collective-permute-start(bf16[4,32,4,128]{3,1,2,0:T(8,128)(2,1)S(1)} %pad_maximum_fusion.4), channel_id=1, source_target_pairs={{0,4},{4,8},{8,12},{12,16},{16,20},{20,24},{24,28},{1,5},{5,9},{9,... | collective-permute-start | bytes 393224 | tf_op jit(solution)/shard_map/ppermute | solution.py:37
  195.2 1.5 collective-permute-start.12
  198.6 3.9 %collective-permute-done.12 = bf16[4,32,4,128]{3,1,2,0:T(8,128)(2,1)S(1)} collective-permute-done((bf16[4,32,4,128]{3,1,2,0:T(8,128)(2,1)S(1)}, bf16[4,32,4,128]{3,1,2,0:T(8,128)(2,1)S(1)}, u32[]{:S(2)}, u32[]{:S(2)}) %collective-permute-start.12) | collective-permute-done | bytes 131104 | tf_op jit(solution)/shard_map/ppermute | solution.py:38
  206.6 7.9 %gather_fusion.2 = f32[1024,4,8]{2,1,0:T(4,128)} fusion(f32[4,8,16]{1,0,2:T(4,128)S(1)} %bitcast.251, s32[1024]{0:T(1024)S(1)} %broadcast_clamp_fusion), kind=kCustom, calls=%fused_computation.2 | custom fusion | bytes 266240 | tf_op jit(solution)/shard_map/gather | solution.py:71
  214.5 2.4 copy.184
  216.9 9.7 %reduce-scatter.6.cloned.1.call-done = bf16[128,256]{1,0:T(8,128)(2,1)} async-done(((bf16[128,1024]{1,0:T(8,128)(2,1)}), bf16[128,256]{1,0:T(8,128)(2,1)}) %reduce-scatter.6.cloned.1.call-update) | async-done | bytes 65552 | tf_op jit(solution)/shard_map/reduce_scatter | solution.py:122
  226.6 6.0 %all_gather.23 = bf16[128,1024]{1,0:T(8,128)(2,1)S(1)} all-gather(bf16[128,256]{1,0:T(8,128)(2,1)} %reduce-scatter.6.cloned.1.call-done), channel_id=1, replica_groups=mesh['sp'=8,'tp'=4] {'tp'}, dimensions={1}, use_global_device_ids=true | all-gather | bytes 327680 | tf_op jit(solution)/shard_map/all_gather | solution.py:100
  236.3 3.4 %collective-permute-start.13 = (bf16[4,32,4,128]{3,1,2,0:T(8,128)(2,1)S(1)}, bf16[4,32,4,128]{3,1,2,0:T(8,128)(2,1)S(1)}, u32[]{:S(2)}, u32[]{:S(2)}) collective-permute-start(bf16[4,32,4,128]{3,1,2,0:T(8,128)(2,1)S(1)} %pad_maximum_fusion.5), channel_id=1, source_target_pairs={{0,4},{4,8},{8,12},{12,16},{16,20},{20,24},{24,28},{1,5},{5,9},{9,... | collective-permute-start | bytes 393224 | tf_op jit(solution)/shard_map/ppermute | solution.py:37
  243.0 4.1 %collective-permute-done.14 = bf16[4,32,4,128]{3,1,2,0:T(8,128)(2,1)S(1)} collective-permute-done((bf16[4,32,4,128]{3,1,2,0:T(8,128)(2,1)S(1)}, bf16[4,32,4,128]{3,1,2,0:T(8,128)(2,1)S(1)}, u32[]{:S(2)}, u32[]{:S(2)}) %collective-permute-start.14) | collective-permute-done | bytes 131104 | tf_op jit(solution)/shard_map/ppermute | solution.py:38
  250.9 20.2 %reduce-scatter.8.cloned.1.call-done = bf16[128,256]{1,0:T(8,128)(2,1)} async-done(((bf16[128,1024]{1,0:T(8,128)(2,1)}), bf16[128,256]{1,0:T(8,128)(2,1)}) %reduce-scatter.8.cloned.1.call-update) | async-done | bytes 65552 | tf_op jit(solution)/shard_map/reduce_scatter | solution.py:122
  (157 shorter events, 35.7 us)
Async XLA Ops:
  6.5 20.1 %copy-start = (bf16[3,256,128]{2,1,0:T(8,128)(2,1)S(1)}, bf16[3,256,128]{2,1,0:T(8,128)(2,1)}, u32[]{:S(2)}) copy-start(bf16[3,256,128]{2,1,0:T(8,128)(2,1)} %param.13) | copy-start | bytes 589828
  6.5 70.2 %all-gather.4.cloned.1.call-start = ((), (), s32[]{:S(2)}) async-start(), calls=%async_computation.3 | async-start | bytes 1769472 | tf_op jit(solution)/shard_map/all_gather | solution.py:94
  7.3 105.8 %all-gather.6.cloned.1.call-start = ((), (), s32[]{:S(2)}) async-start(), calls=%async_computation.4 | async-start | bytes 1769472 | tf_op jit(solution)/shard_map/all_gather | solution.py:95
  8.0 149.7 %all-gather.8.cloned.1.call-start = ((), (), s32[]{:S(2)}) async-start(), calls=%async_computation.5 | async-start | bytes 1769472 | tf_op jit(solution)/shard_map/all_gather | solution.py:93
  8.1 29.4 %collective-permute-start.4 = (bf16[3,256,128]{2,1,0:T(8,128)(2,1)}, bf16[3,256,128]{2,1,0:T(8,128)(2,1)S(1)}, u32[]{:S(2)}, u32[]{:S(2)}) collective-permute-start(bf16[3,256,128]{2,1,0:T(8,128)(2,1)} %param.13), channel_id=1, source_target_pairs={{0,4},{4,8},{8,12},{12,16},{16,20},{20,24},{24,28},{28,0},{1,5},{5... | collective-permute-start | bytes 589832 | tf_op jit(solution)/shard_map/ppermute | solution.py:20
  11.1 29.1 %collective-permute-start.5 = (bf16[3,256,128]{2,1,0:T(8,128)(2,1)}, bf16[3,256,128]{2,1,0:T(8,128)(2,1)S(1)}, u32[]{:S(2)}, u32[]{:S(2)}) collective-permute-start(bf16[3,256,128]{2,1,0:T(8,128)(2,1)} %param.13), channel_id=1, source_target_pairs={{0,28},{4,0},{8,4},{12,8},{16,12},{20,16},{24,20},{28,24},{1,29},{... | collective-permute-start | bytes 589832 | tf_op jit(solution)/shard_map/ppermute | solution.py:23
  14.9 22.2 %collective-permute-start.2 = (s32[4,32]{1,0:T(4,128)S(1)}, s32[4,32]{1,0:T(4,128)S(1)}, u32[]{:S(2)}, u32[]{:S(2)}) collective-permute-start(s32[4,32]{1,0:T(4,128)S(1)} %reshape.186), channel_id=1, source_target_pairs={{0,4},{4,8},{8,12},{12,16},{16,20},{20,24},{24,28},{1,5},{5,9},{9,... | collective-permute-start | bytes 1544 | tf_op jit(solution)/shard_map/ppermute | solution.py:37
  16.2 20.9 %collective-permute-start.3 = (s32[4,32]{1,0:T(4,128)S(1)}, s32[4,32]{1,0:T(4,128)S(1)}, u32[]{:S(2)}, u32[]{:S(2)}) collective-permute-start(s32[4,32]{1,0:T(4,128)S(1)} %reshape.186), channel_id=1, source_target_pairs={{4,0},{8,4},{12,8},{16,12},{20,16},{24,20},{28,24},{5,1},{9,5},{13... | collective-permute-start | bytes 1544 | tf_op jit(solution)/shard_map/ppermute | solution.py:38
  17.5 164.6 %reduce-scatter.4.cloned.1.call-start = ((), (), s32[]{:S(2)}) async-start(), calls=%async_computation.6 | async-start | bytes 327680 | tf_op jit(solution)/shard_map/reduce_scatter | solution.py:122
  37.5 16.2 %collective-permute-start.6 = (bf16[3,256,128]{2,1,0:T(8,128)(2,1)S(1)}, bf16[3,256,128]{2,1,0:T(8,128)(2,1)S(1)}, u32[]{:S(2)}, u32[]{:S(2)}) collective-permute-start(bf16[3,256,128]{2,1,0:T(8,128)(2,1)S(1)} %collective-permute-done.4), channel_id=1, source_target_pairs={{0,4},{4,8},{8,12},{12,16},{16,20},{20,24},{24,28},{28,0},{1,5},{5... | collective-permute-start | bytes 589832 | tf_op jit(solution)/shard_map/ppermute | solution.py:20
  40.2 16.5 %collective-permute-start.7 = (bf16[3,256,128]{2,1,0:T(8,128)(2,1)S(1)}, bf16[3,256,128]{2,1,0:T(8,128)(2,1)S(1)}, u32[]{:S(2)}, u32[]{:S(2)}) collective-permute-start(bf16[3,256,128]{2,1,0:T(8,128)(2,1)S(1)} %collective-permute-done.5), channel_id=1, source_target_pairs={{0,28},{4,0},{8,4},{12,8},{16,12},{20,16},{24,20},{28,24},{1,29},{... | collective-permute-start | bytes 589832 | tf_op jit(solution)/shard_map/ppermute | solution.py:23
  53.7 14.3 %collective-permute-start.8 = (bf16[3,256,128]{2,1,0:T(8,128)(2,1)S(1)}, bf16[3,256,128]{2,1,0:T(8,128)(2,1)S(1)}, u32[]{:S(2)}, u32[]{:S(2)}) collective-permute-start(bf16[3,256,128]{2,1,0:T(8,128)(2,1)S(1)} %collective-permute-done.6), channel_id=1, source_target_pairs={{0,4},{4,8},{8,12},{12,16},{16,20},{20,24},{24,28},{28,0},{1,5},{5... | collective-permute-start | bytes 589832 | tf_op jit(solution)/shard_map/ppermute | solution.py:20
  56.7 11.4 %collective-permute-start.9 = (bf16[3,256,128]{2,1,0:T(8,128)(2,1)S(1)}, bf16[3,256,128]{2,1,0:T(8,128)(2,1)S(1)}, u32[]{:S(2)}, u32[]{:S(2)}) collective-permute-start(bf16[3,256,128]{2,1,0:T(8,128)(2,1)S(1)} %collective-permute-done.7), channel_id=1, source_target_pairs={{0,28},{4,0},{8,4},{12,8},{16,12},{20,16},{24,20},{28,24},{1,29},{... | collective-permute-start | bytes 589832 | tf_op jit(solution)/shard_map/ppermute | solution.py:23
  68.0 8.7 %collective-permute-start.10 = (bf16[3,256,128]{2,1,0:T(8,128)(2,1)S(1)}, bf16[3,256,128]{2,1,0:T(8,128)(2,1)S(1)}, u32[]{:S(2)}, u32[]{:S(2)}) collective-permute-start(bf16[3,256,128]{2,1,0:T(8,128)(2,1)S(1)} %collective-permute-done.8), channel_id=1, source_target_pairs={{0,4},{4,8},{8,12},{12,16},{16,20},{20,24},{24,28},{28,0},{1,5},{5... | collective-permute-start | bytes 589832 | tf_op jit(solution)/shard_map/ppermute | solution.py:20
  114.8 44.8 %collective-permute-start = (bf16[4,32,4,128]{3,1,2,0:T(8,128)(2,1)S(1)}, bf16[4,32,4,128]{3,1,2,0:T(8,128)(2,1)S(1)}, u32[]{:S(2)}, u32[]{:S(2)}) collective-permute-start(bf16[4,32,4,128]{3,1,2,0:T(8,128)(2,1)S(1)} %pad_maximum_fusion.3), channel_id=1, source_target_pairs={{0,4},{4,8},{8,12},{12,16},{16,20},{20,24},{24,28},{1,5},{5,9},{9,... | collective-permute-start | bytes 393224 | tf_op jit(solution)/shard_map/ppermute | solution.py:37
  117.3 42.4 %collective-permute-start.1 = (bf16[4,32,4,128]{3,1,2,0:T(8,128)(2,1)S(1)}, bf16[4,32,4,128]{3,1,2,0:T(8,128)(2,1)S(1)}, u32[]{:S(2)}, u32[]{:S(2)}) collective-permute-start(bf16[4,32,4,128]{3,1,2,0:T(8,128)(2,1)S(1)} %pad_maximum_fusion.3), channel_id=1, source_target_pairs={{4,0},{8,4},{12,8},{16,12},{20,16},{24,20},{28,24},{5,1},{9,5},{13... | collective-permute-start | bytes 393224 | tf_op jit(solution)/shard_map/ppermute | solution.py:38
  163.6 63.1 %reduce-scatter.6.cloned.1.call-start = ((), (), s32[]{:S(2)}) async-start(), calls=%async_computation.7 | async-start | bytes 327680 | tf_op jit(solution)/shard_map/reduce_scatter | solution.py:122
  191.8 6.8 %collective-permute-start.11 = (bf16[4,32,4,128]{3,1,2,0:T(8,128)(2,1)S(1)}, bf16[4,32,4,128]{3,1,2,0:T(8,128)(2,1)S(1)}, u32[]{:S(2)}, u32[]{:S(2)}) collective-permute-start(bf16[4,32,4,128]{3,1,2,0:T(8,128)(2,1)S(1)} %pad_maximum_fusion.4), channel_id=1, source_target_pairs={{0,4},{4,8},{8,12},{12,16},{16,20},{20,24},{24,28},{1,5},{5,9},{9,... | collective-permute-start | bytes 393224 | tf_op jit(solution)/shard_map/ppermute | solution.py:37
  195.2 7.4 %collective-permute-start.12 = (bf16[4,32,4,128]{3,1,2,0:T(8,128)(2,1)S(1)}, bf16[4,32,4,128]{3,1,2,0:T(8,128)(2,1)S(1)}, u32[]{:S(2)}, u32[]{:S(2)}) collective-permute-start(bf16[4,32,4,128]{3,1,2,0:T(8,128)(2,1)S(1)} %pad_maximum_fusion.4), channel_id=1, source_target_pairs={{4,0},{8,4},{12,8},{16,12},{20,16},{24,20},{28,24},{5,1},{9,5},{13... | collective-permute-start | bytes 393224 | tf_op jit(solution)/shard_map/ppermute | solution.py:38
  204.2 2.3 copy-start.1
  206.5 64.7 %reduce-scatter.8.cloned.1.call-start = ((), (), s32[]{:S(2)}) async-start(), calls=%async_computation.8 | async-start | bytes 327680 | tf_op jit(solution)/shard_map/reduce_scatter | solution.py:122
  236.3 6.6 %collective-permute-start.13 = (bf16[4,32,4,128]{3,1,2,0:T(8,128)(2,1)S(1)}, bf16[4,32,4,128]{3,1,2,0:T(8,128)(2,1)S(1)}, u32[]{:S(2)}, u32[]{:S(2)}) collective-permute-start(bf16[4,32,4,128]{3,1,2,0:T(8,128)(2,1)S(1)} %pad_maximum_fusion.5), channel_id=1, source_target_pairs={{0,4},{4,8},{8,12},{12,16},{16,20},{20,24},{24,28},{1,5},{5,9},{9,... | collective-permute-start | bytes 393224 | tf_op jit(solution)/shard_map/ppermute | solution.py:37
  239.7 7.4 %collective-permute-start.14 = (bf16[4,32,4,128]{3,1,2,0:T(8,128)(2,1)S(1)}, bf16[4,32,4,128]{3,1,2,0:T(8,128)(2,1)S(1)}, u32[]{:S(2)}, u32[]{:S(2)}) collective-permute-start(bf16[4,32,4,128]{3,1,2,0:T(8,128)(2,1)S(1)} %pad_maximum_fusion.5), channel_id=1, source_target_pairs={{4,0},{8,4},{12,8},{16,12},{20,16},{24,20},{28,24},{5,1},{9,5},{13... | collective-permute-start | bytes 393224 | tf_op jit(solution)/shard_map/ppermute | solution.py:38
Sparse Core Ops, SparseCore 0:
  9.5 57.4 all-gather.3
  69.2 43.8 all-gather.5
  115.3 42.3 all-gather.7
  163.7 18.4 reduce-scatter.3
  206.6 20.0 reduce-scatter.5
  251.0 20.0 reduce-scatter.7
